TPU v7x, 32 devices: a whole 2x2x4 slice. The times are simulated.
32 devices in a mesh: sp: 8 (over z, y), tp: 4 (over x, core).
Axes of the slice: x: 2, y: 2, z: 4, core: 2. Of those that a mesh axis runs over, the one named last changes fastest.
Arguments:
- residual_in: bfloat16 [3072, 2048], P(('sp', 'tp')), may hold values from -6 to 6
- queries: bfloat16 [3072, 2048], P('sp', 'tp'), may hold values from -180 to 180
- keys: bfloat16 [3072, 2048], P('sp', 'tp'), may hold values from -9 to 9
- values: bfloat16 [3072, 2048], P('sp', 'tp'), may hold values from -6 to 6
- mix_lambda: float32 [16], P('tp'), may hold values from 0.3 to 0.8
- head_gain: float32 [128], replicated, may hold values from 0.1 to 1.9
- out_weight: bfloat16 [2048, 2048], P('tp'), may hold values from -0.125 to 0.125
- norm_gain: float32 [2048], replicated, may hold values from 0.1 to 1.9
- gate_weight: bfloat16 [2048, 5632], P('sp', 'tp'), may hold values from -0.125 to 0.125
- up_weight: bfloat16 [2048, 5632], P('sp', 'tp'), may hold values from -0.125 to 0.125
- down_weight: bfloat16 [5632, 2048], P('tp', 'sp'), may hold values from -0.078125 to 0.078125
Outputs:
- layer_out: bfloat16 [3072, 2048], P(('sp', 'tp'))
All inputs are finite; a program needn't handle non-finite values.
Results may differ from a plain program's by a relative error of at most 0.014.
Values may be sent and summed in bfloat16 or wider, within the bound.
A program may use at most 128 MiB of HBM per device.

v0:
```python
import math
import jax
import jax.numpy as jnp
from jax import lax
from jax.sharding import PartitionSpec as P

DH = 64
VD = 128


def body(
    residual_in,
    queries,
    keys,
    values,
    mix_lambda,
    head_gain,
    out_weight,
    norm_gain,
    gate_weight,
    up_weight,
    down_weight,
):
    tp_count = lax.axis_size("tp")
    tok_local = queries.shape[0]
    heads_local = mix_lambda.shape[0]
    rows_local = tok_local // tp_count
    query_four = queries.reshape(tok_local, heads_local, 2, DH)
    inverse_root = 1.0 / math.sqrt(DH)

    def one_block(state, block):
        top, total, weighted = state
        key_block, value_block = block
        scores = (
            jnp.einsum("qhcd,khcd->hcqk", query_four, key_block, preferred_element_type=jnp.float32)
            * inverse_root
        )
        new_top = jnp.maximum(top, jnp.max(scores, axis=-1))
        rescale = jnp.exp(top - new_top)
        expo = jnp.exp(scores - new_top[..., None])
        total = total * rescale + jnp.sum(expo, axis=-1)
        weighted = weighted * rescale[..., None] + jnp.einsum(
            "hcqk,khe->hcqe",
            expo.astype(jnp.bfloat16),
            value_block,
            preferred_element_type=jnp.float32,
        )
        return ((new_top, total, weighted), None)

    start_state = (
        jnp.full((heads_local, 2, tok_local), -1e30, jnp.float32),
        jnp.zeros((heads_local, 2, tok_local), jnp.float32),
        jnp.zeros((heads_local, 2, tok_local, VD), jnp.float32),
    )
    key_piece = lax.all_gather(keys, "sp", axis=0, tiled=True)
    value_piece = lax.all_gather(values, "sp", axis=0, tiled=True)
    count = key_piece.shape[0]
    shards = max(count // tok_local, 1)
    unit = count // shards
    group = max(
        (g for g in range(1, shards + 1) if shards % g == 0 and g * unit <= max(1536, unit))
    )
    width = group * unit
    blocks = count // width
    key_blocks = key_piece.reshape(blocks, width, heads_local, 2, DH)
    value_blocks = value_piece.reshape(blocks, width, heads_local, VD)
    state, unused = lax.scan(one_block, start_state, (key_blocks, value_blocks))
    top, total, weighted = state
    maps = weighted / total[..., None]
    mixed = maps[:, 0] - mix_lambda[:, None, None] * maps[:, 1]
    head_scale = lax.rsqrt(jnp.mean(mixed * mixed, axis=-1, keepdims=True) + 1e-06)
    head_out = (mixed * head_scale * head_gain).astype(jnp.bfloat16)
    attended = jnp.transpose(head_out, (1, 0, 2)).reshape(tok_local, heads_local * VD)
    summed = lax.psum(
        jnp.dot(attended, out_weight, preferred_element_type=jnp.float32).astype(jnp.bfloat16), "tp"
    ).astype(jnp.float32)
    residual_all = lax.all_gather(residual_in, "tp", axis=0, tiled=True)
    after_all = residual_all.astype(jnp.float32) + summed
    row_scale = lax.rsqrt(jnp.mean(after_all * after_all, axis=-1, keepdims=True) + 1e-06)
    all_rows = (after_all * row_scale * norm_gain).astype(jnp.bfloat16)
    after_mix = lax.dynamic_slice_in_dim(
        after_all, lax.axis_index("tp") * rows_local, rows_local, 0
    )
    gate_all, up_all, down_all = (
        lax.all_gather(gate_weight, "sp", axis=0, tiled=True),
        lax.all_gather(up_weight, "sp", axis=0, tiled=True),
        lax.all_gather(down_weight, "sp", axis=1, tiled=True),
    )
    gate = jnp.dot(all_rows, gate_all, preferred_element_type=jnp.float32)
    up = jnp.dot(all_rows, up_all, preferred_element_type=jnp.float32)
    hidden = (jax.nn.silu(gate) * up).astype(jnp.bfloat16)
    mixer = lax.psum_scatter(
        jnp.dot(hidden, down_all, preferred_element_type=jnp.float32).astype(jnp.bfloat16),
        "tp",
        scatter_dimension=0,
        tiled=True,
    ).astype(jnp.float32)
    return (after_mix + 0.5 * mixer).astype(jnp.bfloat16)


def solution(mesh):
    return jax.shard_map(
        body,
        mesh=mesh,
        in_specs=(
            P(("sp", "tp"), None),
            P("sp", "tp"),
            P("sp", "tp"),
            P("sp", "tp"),
            P("tp"),
            P(),
            P("tp", None),
            P(),
            P("sp", "tp"),
            P("sp", "tp"),
            P("tp", "sp"),
        ),
        out_specs=P(("sp", "tp"), None),
        check_vma=False,
    )
```

profile of v0, /device:TPU:0, one launch (start us, length us, event | category | flops | bytes accessed | tf_op | source)
XLA Modules:
  0.0 579.6 jit_solution(15325134770839630398)
XLA Ops:
  6.5 0.7 all-gather.9.cloned.1.call-update
  7.3 0.7 all-gather.11.cloned.1.call-update
  8.8 1.2 copy.17
  10.0 62.3 %all-gather.9.cloned.1.call-done = bf16[3072,512]{1,0:T(8,128)(2,1)} async-done(((bf16[384,512]{1,0:T(8,128)(2,1)}), bf16[3072,512]{1,0:T(8,128)(2,1)}) %all-gather.9.cloned.1.call-update) | async-done | bytes 3145744 | tf_op jit(solution)/shard_map/all_gather | solution.py:55
  72.3 12.5 %reshape.39 = bf16[2,1536,4,2,64]{4,3,2,1,0:T(2,128)(2,1)} reshape(bf16[3072,512]{1,0:T(8,128)(2,1)} %all-gather.9.cloned.1.call-done) | data formatting | bytes 6291456 | tf_op jit(solution)/shard_map/reshape | solution.py:65
  84.8 15.4 %copy.18 = bf16[2,1536,4,2,64]{1,4,3,2,0:T(8,128)(2,1)} copy(bf16[2,1536,4,2,64]{4,3,2,1,0:T(2,128)(2,1)} %reshape.39) | data formatting | bytes 6291456
  100.2 33.0 %all-gather.11.cloned.1.call-done = bf16[3072,512]{1,0:T(8,128)(2,1)} async-done(((bf16[384,512]{1,0:T(8,128)(2,1)}), bf16[3072,512]{1,0:T(8,128)(2,1)}) %all-gather.11.cloned.1.call-update) | async-done | bytes 3145744 | tf_op jit(solution)/shard_map/all_gather | solution.py:56
  133.2 5.6 reshape.36
  138.7 63.8 %while.15 = (s32[]{:T(128)}, f32[4,2,384]{2,1,0:T(2,128)S(1)}, f32[4,2,384]{2,1,0:T(2,128)S(1)}, f32[4,2,384,128]{3,2,1,0:T(8,128)}, bf16[2,1536,4,2,64]{1,4,3,2...) while((s32[]{:T(128)}, f32[4,2,384]{2,1,0:T(2,128)S(1)}, ...), condition=%wide.region_3.4_spmd.clone, body=%wide.region_0.3_spmd.clone.sunk | while | flops 1850883072 | bytes 79233688 | solution.py:67
  138.7 10.6 %bitcast_reduce_fusion.2 = (f32[4,2,384]{2,1,0:T(2,128)S(1)}, f32[4,2,1536,384]{3,2,1,0:T(8,128)}) fusion(bf16[384,4,2,64]{0,3,2,1:T(8,128)(2,1)S(1)} %get-tuple-element.170, bf16[2,1536,4,2,64]{1,4,3,2,0:T(8,128)(2,1)} %get-tuple-element.169, s32[]{:T(128)} %get-tuple-element.156), kind=kOutput, calls=%fused_computation.1.clone.1 | convolution fusion | flops 613413888 | bytes 20853248 | tf_op jit(solution)/shard_map/while/body/eval_jaxpr/qhcd,khcd->hcqk/dot_general | solution.py:35
  149.4 9.5 %fusion.37 = f32[4,2,384]{2,1,0:T(2,128)S(1)} fusion(f32[4,2,1536,384]{3,2,1,0:T(8,128)} %get-tuple-element.144, f32[4,2,384]{2,1,0:T(2,128)S(1)} %fusion.36), kind=kLoop, calls=%fused_computation.4.clone.1 | loop fusion | flops 14152704 | bytes 18898944 | tf_op jit(solution)/shard_map/while/body/eval_jaxpr/reduce_sum | solution.py:41
  158.9 1.8 constant_dynamic-slice_fusion.2
  160.7 8.8 %fusion.39 = f32[4,2,384,128]{3,2,1,0:T(8,128)S(1)} fusion(f32[4,2,384,128]{3,2,1,0:T(8,128)S(1)} %copy-done.1, bf16[1,1536,4,128]{3,2,1,0:T(4,128)(2,1)S(1)} %constant_dynamic-slice_fusion.2, f32[4,2,1536,384]{3,2,1,0:T(8,128)} %get-tuple-element.144, f32[4,2,384]{2,1,0:T(2,128)S(1)} %fusion.36, f32[4,2,384]{2,1,0:T(2,128)S(1)} %get-tuple-element.146, ...), kind=kOutput, calls=%fused_computation.12.clone.1 | convolution fusion | flops 1223294976 | bytes 23617536 | tf_op jit(solution)/shard_map/while/body/eval_jaxpr/hcqk,khe->hcqe/dot_general | solution.py:42
  169.5 1.1 copy-done.2
  170.7 10.5 %bitcast_reduce_fusion.2 = (f32[4,2,384]{2,1,0:T(2,128)S(1)}, f32[4,2,1536,384]{3,2,1,0:T(8,128)}) fusion(bf16[384,4,2,64]{0,3,2,1:T(8,128)(2,1)S(1)} %get-tuple-element.170, bf16[2,1536,4,2,64]{1,4,3,2,0:T(8,128)(2,1)} %get-tuple-element.169, s32[]{:T(128)} %get-tuple-element.156), kind=kOutput, calls=%fused_computation.1.clone.1 | convolution fusion | flops 613413888 | bytes 20853248 | tf_op jit(solution)/shard_map/while/body/eval_jaxpr/qhcd,khcd->hcqk/dot_general | solution.py:35
  181.2 9.4 %fusion.37 = f32[4,2,384]{2,1,0:T(2,128)S(1)} fusion(f32[4,2,1536,384]{3,2,1,0:T(8,128)} %get-tuple-element.144, f32[4,2,384]{2,1,0:T(2,128)S(1)} %fusion.36), kind=kLoop, calls=%fused_computation.4.clone.1 | loop fusion | flops 14152704 | bytes 18898944 | tf_op jit(solution)/shard_map/while/body/eval_jaxpr/reduce_sum | solution.py:41
  190.7 1.8 constant_dynamic-slice_fusion.2
  192.6 8.8 %fusion.39 = f32[4,2,384,128]{3,2,1,0:T(8,128)S(1)} fusion(f32[4,2,384,128]{3,2,1,0:T(8,128)S(1)} %copy-done.1, bf16[1,1536,4,128]{3,2,1,0:T(4,128)(2,1)S(1)} %constant_dynamic-slice_fusion.2, f32[4,2,1536,384]{3,2,1,0:T(8,128)} %get-tuple-element.144, f32[4,2,384]{2,1,0:T(2,128)S(1)} %fusion.36, f32[4,2,384]{2,1,0:T(2,128)S(1)} %get-tuple-element.146, ...), kind=kOutput, calls=%fused_computation.12.clone.1 | convolution fusion | flops 1223294976 | bytes 23617536 | tf_op jit(solution)/shard_map/while/body/eval_jaxpr/hcqk,khe->hcqe/dot_general | solution.py:42
  201.4 1.1 copy-done.2
  202.5 3.1 copy.21
  205.6 1.5 broadcast_divide_fusion
  207.6 2.2 convolution_convert_fusion.1
  211.0 0.7 all-gather.17.cloned.1.call-update
  211.8 39.7 %all-reduce.2.cloned.1.call-done = bf16[384,2048]{1,0:T(8,128)(2,1)} async-done(((bf16[384,2048]{1,0:T(8,128)(2,1)}), bf16[384,2048]{1,0:T(8,128)(2,1)}) %all-reduce.2.cloned.1.call-update) | async-done | bytes 1572880 | tf_op jit(solution)/shard_map/psum | solution.py:74
  251.5 4.0 convert_add_fusion
  255.5 90.4 %all-gather.13.cloned.1.call-done = bf16[2048,1408]{1,0:T(8,128)(2,1)} async-done(((bf16[256,1408]{1,0:T(8,128)(2,1)}), bf16[2048,1408]{1,0:T(8,128)(2,1)}) %all-gather.13.cloned.1.call-update) | async-done | bytes 5767184 | tf_op jit(solution)/shard_map/all_gather | solution.py:85
  345.9 7.6 %fusion.21 = f32[384,1408]{1,0:T(8,128)} fusion(bf16[2048,1408]{1,0:T(8,128)(2,1)} %all-gather.13.cloned.1.call-done, f32[2048]{0:T(1024)S(1)} %copy-done.5, f32[384]{0:T(512)S(1)} %add_rsqrt_fusion.1, bf16[384,2048]{1,0:T(8,128)(2,1)} %all-reduce.2.cloned.1.call-done, bf16[384,2048]{1,0:T(8,128)(2,1)} %all-gather.7.cloned.1.call-done), kind=kOutput, calls=%fused_computation.40 | convolution fusion | flops 2219311104 | bytes 11085312 | tf_op jit(solution)/shard_map/dot_general | solution.py:89
  353.5 85.0 %all-gather.15.cloned.1.call-done = bf16[2048,1408]{1,0:T(8,128)(2,1)} async-done(((bf16[256,1408]{1,0:T(8,128)(2,1)}), bf16[2048,1408]{1,0:T(8,128)(2,1)}) %all-gather.15.cloned.1.call-update) | async-done | bytes 5767184 | tf_op jit(solution)/shard_map/all_gather | solution.py:86
  438.5 93.4 %all-gather.17.cloned.1.call-done = bf16[1408,2048]{1,0:T(8,128)(2,1)} async-done(((bf16[1408,256]{1,0:T(8,128)(2,1)}), bf16[1408,2048]{1,0:T(8,128)(2,1)}) %all-gather.17.cloned.1.call-update) | async-done | bytes 5767184 | tf_op jit(solution)/shard_map/all_gather | solution.py:87
  531.9 12.4 %convolution_convert_fusion = bf16[384,2048]{1,0:T(8,128)(2,1)} fusion(bf16[1408,2048]{1,0:T(8,128)(2,1)} %all-gather.17.cloned.1.call-done, bf16[2048,1408]{1,0:T(8,128)(2,1)} %all-gather.15.cloned.1.call-done, f32[384,1408]{1,0:T(8,128)} %fusion.21, f32[2048]{0:T(1024)S(1)} %copy-done.5, f32[384]{0:T(512)S(1)} %add_rsqrt_fusion.1, ...), kind=kOutput, calls=%fused_computation.27 | convolution fusion | flops 4437934080 | bytes 18425344 | tf_op jit(solution)/shard_map/dot_general | solution.py:93
  544.3 26.4 %reduce-scatter.2.cloned.1.call-done = bf16[96,2048]{1,0:T(8,128)(2,1)} async-done(((bf16[384,2048]{1,0:T(8,128)(2,1)}), bf16[96,2048]{1,0:T(8,128)(2,1)}) %reduce-scatter.2.cloned.1.call-update) | async-done | bytes 393232 | tf_op jit(solution)/shard_map/reduce_scatter | solution.py:92
  570.7 2.1 add_convert_fusion
  (42 shorter events, 2.6 us)
Async XLA Ops:
  6.5 201.0 %copy-start = (bf16[512,2048]{1,0:T(8,128)(2,1)S(1)}, bf16[512,2048]{1,0:T(8,128)(2,1)}, u32[]{:S(2)}) copy-start(bf16[512,2048]{1,0:T(8,128)(2,1)} %param.19) | copy-start | bytes 6291460
  6.5 65.8 %all-gather.9.cloned.1.call-start = ((), (), s32[]{:S(2)}) async-start(), calls=%async_computation.2 | async-start | bytes 3538944 | tf_op jit(solution)/shard_map/all_gather | solution.py:55
  7.3 125.9 %all-gather.11.cloned.1.call-start = ((), (), s32[]{:S(2)}) async-start(), calls=%async_computation.3 | async-start | bytes 3538944 | tf_op jit(solution)/shard_map/all_gather | solution.py:56
  8.0 203.8 %all-gather.7.cloned.1.call-start = ((), (), s32[]{:S(2)}) async-start(), calls=%async_computation.1 | async-start | bytes 1966080 | tf_op jit(solution)/shard_map/all_gather | solution.py:77
  8.7 242.7 %all-reduce.2.cloned.1.call-start = ((), (), s32[]{:S(2)}) async-start(), calls=%async_computation.4 | async-start | bytes 3145728 | tf_op jit(solution)/shard_map/psum | solution.py:74
  158.8 1.9 copy-start.1
  169.5 1.1 copy-start.2
  190.7 1.9 copy-start.1
  201.3 1.1 copy-start.2
  205.6 1.6 copy-start.3
  205.6 1.8 copy-start.4
  209.8 136.1 %all-gather.13.cloned.1.call-start = ((), (), s32[]{:S(2)}) async-start(), calls=%async_computation.5 | async-start | bytes 6488064 | tf_op jit(solution)/shard_map/all_gather | solution.py:85
  210.4 228.1 %all-gather.15.cloned.1.call-start = ((), (), s32[]{:S(2)}) async-start(), calls=%async_computation.6 | async-start | bytes 6488064 | tf_op jit(solution)/shard_map/all_gather | solution.py:86
  210.9 321.0 %all-gather.17.cloned.1.call-start = ((), (), s32[]{:S(2)}) async-start(), calls=%async_computation.7 | async-start | bytes 6488064 | tf_op jit(solution)/shard_map/all_gather | solution.py:87
  211.7 134.2 %copy-start.5 = (f32[2048]{0:T(1024)S(1)}, f32[2048]{0:T(1024)}, u32[]{:S(2)}) copy-start(f32[2048]{0:T(1024)} %param.20) | copy-start | bytes 24580
  211.7 359.0 %reduce-scatter.2.cloned.1.call-start = ((), (), s32[]{:S(2)}) async-start(), calls=%async_computation.8 | async-start | bytes 1966080 | tf_op jit(solution)/shard_map/reduce_scatter | solution.py:92
Sparse Core Ops, SparseCore 0:
  9.5 62.7 all-gather.8
  74.5 58.6 all-gather.10
  134.7 18.2 all-gather.6
  209.9 41.5 all-reduce.1
  253.5 92.3 all-gather.12
  347.9 90.5 all-gather.14
  440.5 91.2 all-gather.16
  544.4 26.2 reduce-scatter.1
where the time goes:
time: 581 us; the launch traced here: 580 us
  waiting for transfers between devices  434 us (75%)
  matrix products  60.9 us (10%)
  local copies, waits for them, and re-layouts  43.7 us (8%)
  other arithmetic  27.1 us (5%)
  between operations  13.6 us (2%)
    all_gather x1, waiting for transfers between devices, body(): lax.all_gather(down_weight, 'sp', axis=1, tiled=True)  93.4 us
    all_gather x1, waiting for transfers between devices, body(): lax.all_gather(gate_weight, 'sp', axis=0, tiled=True)  90.4 us
    all_gather x1, waiting for transfers between devices, body(): lax.all_gather(up_weight, 'sp', axis=0, tiled=True)  85 us
    all_gather x1, waiting for transfers between devices, body(): key_piece = lax.all_gather(keys, 'sp', axis=0, tiled=True)  62.3 us
    psum x1, waiting for transfers between devices, body(): lax.psum(jnp.dot(attended, out_weight, preferred_element_type=jnp.float32...  39.7 us
    all_gather x1, waiting for transfers between devices, body(): value_piece = lax.all_gather(values, 'sp', axis=0, tiled=True)  33 us
    reduce_scatter x1, waiting for transfers between devices, body(): lax.psum_scatter(jnp.dot(hidden, down_all, preferred_element_type=jnp.flo...  26.4 us
    dot_general x2, matrix products, one_block(): jnp.einsum('qhcd,khcd->hcqk', query_four, key_block, preferred_element_ty...  21.1 us
  transfers between devices with their start and end apart: 8, of which 7 were waited for; matrix products, arithmetic and copies ran while one was open for 20% of the time, Pallas kernels for 0%

commit v1 on v0

--- a/solution.py
+++ b/solution.py
@@ -6,6 +6,19 @@
 
 DH = 64
 VD = 128
+
+
+def link_runs_for(packet, in_dim):
+    outer = jnp.concatenate(
+        jax.lax.all_to_all(
+            jnp.stack([packet for _ in range(jax.lax.axis_size("sp"))]),
+            axis_name="sp",
+            split_axis=0,
+            concat_axis=0,
+        ),
+        axis=in_dim,
+    )
+    return outer
 
 
 def body(
@@ -84,7 +97,7 @@
     gate_all, up_all, down_all = (
         lax.all_gather(gate_weight, "sp", axis=0, tiled=True),
         lax.all_gather(up_weight, "sp", axis=0, tiled=True),
-        lax.all_gather(down_weight, "sp", axis=1, tiled=True),
+        link_runs_for(down_weight, 1),
     )
     gate = jnp.dot(all_rows, gate_all, preferred_element_type=jnp.float32)
     up = jnp.dot(all_rows, up_all, preferred_element_type=jnp.float32)

time: 581 us -> 557 us (0.959)
  waiting for transfers between devices: 434 us -> 402 us
    all_gather x1 -> x0, waiting for transfers between devices: 93.4 us -> none  [body(): lax.all_gather(down_weight, 'sp', axis=1, tiled=True)]
    all_gather x1, waiting for transfers between devices: 90.4 us -> 159 us  [body(): lax.all_gather(gate_weight, 'sp', axis=0, tiled=True)]
    psum x1, waiting for transfers between devices: 39.7 us -> 32 us  [body(): lax.psum(jnp.dot(attended, out_weight, preferred_element_type=jnp.float32...]
    unnamed x10 -> x13, local copies, waits for them, and re-layouts: 16.7 us -> 17.5 us
  transfers between devices with their start and end apart: 8 -> 8, of which waited for: 7 -> 6; matrix products, arithmetic and copies ran while one was open for 20% -> 21% of each run, Pallas kernels for 0% -> 0%
where the time goes in v1:
time: 557 us; the launch traced here: 556 us
  waiting for transfers between devices  402 us (72%)
  matrix products  60.8 us (11%)
  local copies, waits for them, and re-layouts  47.6 us (9%)
  other arithmetic  27.2 us (5%)
  between operations  13.6 us (2%)
    all_gather x1, waiting for transfers between devices, body(): lax.all_gather(gate_weight, 'sp', axis=0, tiled=True)  159 us
    all_gather x1, waiting for transfers between devices, body(): lax.all_gather(up_weight, 'sp', axis=0, tiled=True)  85.5 us
    all_gather x1, waiting for transfers between devices, body(): key_piece = lax.all_gather(keys, 'sp', axis=0, tiled=True)  62.3 us
    all_gather x1, waiting for transfers between devices, body(): value_piece = lax.all_gather(values, 'sp', axis=0, tiled=True)  33 us
    psum x1, waiting for transfers between devices, body(): lax.psum(jnp.dot(attended, out_weight, preferred_element_type=jnp.float32...  32 us
    reduce_scatter x1, waiting for transfers between devices, body(): lax.psum_scatter(jnp.dot(hidden, down_all, preferred_element_type=jnp.flo...  26.4 us
    dot_general x2, matrix products, one_block(): jnp.einsum('qhcd,khcd->hcqk', query_four, key_block, preferred_element_ty...  21.1 us
    reduce_sum x2, other arithmetic, one_block(): total = total * rescale + jnp.sum(expo, axis=-1)  18.9 us
  transfers between devices with their start and end apart: 8, of which 6 were waited for; matrix products, arithmetic and copies ran while one was open for 21% of the time, Pallas kernels for 0%

profile of v1, /device:TPU:0, one launch (start us, length us, event | category | flops | bytes accessed | tf_op | source)
XLA Modules:
  0.0 555.7 jit_solution(18149851041746697276)
XLA Ops:
  6.5 0.7 all-gather.8.cloned.1.call-update
  7.3 0.7 all-gather.10.cloned.1.call-update
  8.8 1.2 copy.17
  10.0 62.3 %all-gather.8.cloned.1.call-done = bf16[3072,512]{1,0:T(8,128)(2,1)} async-done(((bf16[384,512]{1,0:T(8,128)(2,1)}), bf16[3072,512]{1,0:T(8,128)(2,1)}) %all-gather.8.cloned.1.call-update) | async-done | bytes 3145744 | tf_op jit(solution)/shard_map/all_gather | solution.py:68
  72.3 12.5 %reshape.49 = bf16[2,1536,4,2,64]{4,3,2,1,0:T(2,128)(2,1)} reshape(bf16[3072,512]{1,0:T(8,128)(2,1)} %all-gather.8.cloned.1.call-done) | data formatting | bytes 6291456 | tf_op jit(solution)/shard_map/reshape | solution.py:78
  84.8 15.4 %copy.18 = bf16[2,1536,4,2,64]{1,4,3,2,0:T(8,128)(2,1)} copy(bf16[2,1536,4,2,64]{4,3,2,1,0:T(2,128)(2,1)} %reshape.49) | data formatting | bytes 6291456
  100.2 33.0 %all-gather.10.cloned.1.call-done = bf16[3072,512]{1,0:T(8,128)(2,1)} async-done(((bf16[384,512]{1,0:T(8,128)(2,1)}), bf16[3072,512]{1,0:T(8,128)(2,1)}) %all-gather.10.cloned.1.call-update) | async-done | bytes 3145744 | tf_op jit(solution)/shard_map/all_gather | solution.py:69
  133.2 5.6 %reshape.44 = bf16[2,1536,4,128]{3,2,1,0:T(4,128)(2,1)} reshape(bf16[3072,512]{1,0:T(8,128)(2,1)} %all-gather.10.cloned.1.call-done) | data formatting | bytes 6291456 | tf_op jit(solution)/shard_map/reshape | solution.py:79
  138.7 63.9 %while.15 = (s32[]{:T(128)}, f32[4,2,384]{2,1,0:T(2,128)S(1)}, f32[4,2,384]{2,1,0:T(2,128)S(1)}, f32[4,2,384,128]{3,2,1,0:T(8,128)}, bf16[2,1536,4,2,64]{1,4,3,2...) while((s32[]{:T(128)}, f32[4,2,384]{2,1,0:T(2,128)S(1)}, ...), condition=%wide.region_3.4_spmd.clone, body=%wide.region_0.3_spmd.clone.sunk | while | flops 1850883072 | bytes 79233688 | solution.py:80
  138.7 10.6 %bitcast_reduce_fusion.2 = (f32[4,2,384]{2,1,0:T(2,128)S(1)}, f32[4,2,1536,384]{3,2,1,0:T(8,128)}) fusion(bf16[384,4,2,64]{0,3,2,1:T(8,128)(2,1)S(1)} %get-tuple-element.170, bf16[2,1536,4,2,64]{1,4,3,2,0:T(8,128)(2,1)} %get-tuple-element.169, s32[]{:T(128)} %get-tuple-element.156), kind=kOutput, calls=%fused_computation.1.clone.1 | convolution fusion | flops 613413888 | bytes 20853248 | tf_op jit(solution)/shard_map/while/body/eval_jaxpr/qhcd,khcd->hcqk/dot_general | solution.py:48
  149.4 9.5 %fusion.37 = f32[4,2,384]{2,1,0:T(2,128)S(1)} fusion(f32[4,2,1536,384]{3,2,1,0:T(8,128)} %get-tuple-element.144, f32[4,2,384]{2,1,0:T(2,128)S(1)} %fusion.36), kind=kLoop, calls=%fused_computation.4.clone.1 | loop fusion | flops 14152704 | bytes 18898944 | tf_op jit(solution)/shard_map/while/body/eval_jaxpr/reduce_sum | solution.py:54
  158.9 1.8 constant_dynamic-slice_fusion.2
  160.7 8.8 %fusion.39 = f32[4,2,384,128]{3,2,1,0:T(8,128)S(1)} fusion(f32[4,2,384,128]{3,2,1,0:T(8,128)S(1)} %copy-done.1, bf16[1,1536,4,128]{3,2,1,0:T(4,128)(2,1)S(1)} %constant_dynamic-slice_fusion.2, f32[4,2,1536,384]{3,2,1,0:T(8,128)} %get-tuple-element.144, f32[4,2,384]{2,1,0:T(2,128)S(1)} %fusion.36, f32[4,2,384]{2,1,0:T(2,128)S(1)} %get-tuple-element.146, ...), kind=kOutput, calls=%fused_computation.12.clone.1 | convolution fusion | flops 1223294976 | bytes 23617536 | tf_op jit(solution)/shard_map/while/body/eval_jaxpr/hcqk,khe->hcqe/dot_general | solution.py:55
  169.5 1.2 copy-done.2
  170.7 10.5 %bitcast_reduce_fusion.2 = (f32[4,2,384]{2,1,0:T(2,128)S(1)}, f32[4,2,1536,384]{3,2,1,0:T(8,128)}) fusion(bf16[384,4,2,64]{0,3,2,1:T(8,128)(2,1)S(1)} %get-tuple-element.170, bf16[2,1536,4,2,64]{1,4,3,2,0:T(8,128)(2,1)} %get-tuple-element.169, s32[]{:T(128)} %get-tuple-element.156), kind=kOutput, calls=%fused_computation.1.clone.1 | convolution fusion | flops 613413888 | bytes 20853248 | tf_op jit(solution)/shard_map/while/body/eval_jaxpr/qhcd,khcd->hcqk/dot_general | solution.py:48
  181.3 9.4 %fusion.37 = f32[4,2,384]{2,1,0:T(2,128)S(1)} fusion(f32[4,2,1536,384]{3,2,1,0:T(8,128)} %get-tuple-element.144, f32[4,2,384]{2,1,0:T(2,128)S(1)} %fusion.36), kind=kLoop, calls=%fused_computation.4.clone.1 | loop fusion | flops 14152704 | bytes 18898944 | tf_op jit(solution)/shard_map/while/body/eval_jaxpr/reduce_sum | solution.py:54
  190.8 1.8 constant_dynamic-slice_fusion.2
  192.6 8.8 %fusion.39 = f32[4,2,384,128]{3,2,1,0:T(8,128)S(1)} fusion(f32[4,2,384,128]{3,2,1,0:T(8,128)S(1)} %copy-done.1, bf16[1,1536,4,128]{3,2,1,0:T(4,128)(2,1)S(1)} %constant_dynamic-slice_fusion.2, f32[4,2,1536,384]{3,2,1,0:T(8,128)} %get-tuple-element.144, f32[4,2,384]{2,1,0:T(2,128)S(1)} %fusion.36, f32[4,2,384]{2,1,0:T(2,128)S(1)} %get-tuple-element.146, ...), kind=kOutput, calls=%fused_computation.12.clone.1 | convolution fusion | flops 1223294976 | bytes 23617536 | tf_op jit(solution)/shard_map/while/body/eval_jaxpr/hcqk,khe->hcqe/dot_general | solution.py:55
  201.4 1.2 copy-done.2
  202.6 3.0 copy.21
  205.6 1.5 broadcast_divide_fusion
  207.6 2.2 convolution_convert_fusion.1
  211.3 2.9 stack.2
  214.2 4.7 all-to-all-start
  219.6 32.0 %all-reduce.2.cloned.1.call-done = bf16[384,2048]{1,0:T(8,128)(2,1)} async-done(((bf16[384,2048]{1,0:T(8,128)(2,1)}), bf16[384,2048]{1,0:T(8,128)(2,1)}) %all-reduce.2.cloned.1.call-update) | async-done | bytes 1572880 | tf_op jit(solution)/shard_map/psum | solution.py:87
  251.5 4.1 convert_add_fusion
  255.6 159.3 %all-gather.12.cloned.1.call-done = bf16[2048,1408]{1,0:T(8,128)(2,1)} async-done(((bf16[256,1408]{1,0:T(8,128)(2,1)}), bf16[2048,1408]{1,0:T(8,128)(2,1)}) %all-gather.12.cloned.1.call-update) | async-done | bytes 5767184 | tf_op jit(solution)/shard_map/all_gather | solution.py:98
  414.9 7.7 %fusion.21 = f32[384,1408]{1,0:T(8,128)} fusion(bf16[2048,1408]{1,0:T(8,128)(2,1)} %all-gather.12.cloned.1.call-done, f32[2048]{0:T(1024)S(1)} %copy-done.6, f32[384]{0:T(512)S(1)} %add_rsqrt_fusion.1, bf16[384,2048]{1,0:T(8,128)(2,1)} %all-reduce.2.cloned.1.call-done, bf16[384,2048]{1,0:T(8,128)(2,1)} %all-gather.6.cloned.1.call-done), kind=kOutput, calls=%fused_computation.40 | convolution fusion | flops 2219311104 | bytes 11085312 | tf_op jit(solution)/shard_map/dot_general | solution.py:102
  422.6 85.5 %all-gather.14.cloned.1.call-done = bf16[2048,1408]{1,0:T(8,128)(2,1)} async-done(((bf16[256,1408]{1,0:T(8,128)(2,1)}), bf16[2048,1408]{1,0:T(8,128)(2,1)}) %all-gather.14.cloned.1.call-update) | async-done | bytes 5767184 | tf_op jit(solution)/shard_map/all_gather | solution.py:99
  508.1 12.2 %convolution_convert_fusion = bf16[384,2048]{1,0:T(8,128)(2,1)} fusion(bf16[1408,2048]{0,1:T(8,128)(2,1)} %bitcast.6, bf16[2048,1408]{1,0:T(8,128)(2,1)} %all-gather.14.cloned.1.call-done, f32[384,1408]{1,0:T(8,128)} %fusion.21, f32[2048]{0:T(1024)S(1)} %copy-done.6, f32[384]{0:T(512)S(1)} %add_rsqrt_fusion.1, ...), kind=kOutput, calls=%fused_computation.27 | convolution fusion | flops 4437934080 | bytes 18425344 | tf_op jit(solution)/shard_map/dot_general | solution.py:106
  520.4 26.4 %reduce-scatter.2.cloned.1.call-done = bf16[96,2048]{1,0:T(8,128)(2,1)} async-done(((bf16[384,2048]{1,0:T(8,128)(2,1)}), bf16[96,2048]{1,0:T(8,128)(2,1)}) %reduce-scatter.2.cloned.1.call-update) | async-done | bytes 393232 | tf_op jit(solution)/shard_map/reduce_scatter | solution.py:105
  546.8 2.1 add_convert_fusion
  (45 shorter events, 3.4 us)
Async XLA Ops:
  6.5 201.1 %copy-start = (bf16[512,2048]{1,0:T(8,128)(2,1)S(1)}, bf16[512,2048]{1,0:T(8,128)(2,1)}, u32[]{:S(2)}) copy-start(bf16[512,2048]{1,0:T(8,128)(2,1)} %param.19) | copy-start | bytes 6291460
  6.5 65.8 %all-gather.8.cloned.1.call-start = ((), (), s32[]{:S(2)}) async-start(), calls=%async_computation.3 | async-start | bytes 3538944 | tf_op jit(solution)/shard_map/all_gather | solution.py:68
  7.3 125.9 %all-gather.10.cloned.1.call-start = ((), (), s32[]{:S(2)}) async-start(), calls=%async_computation.4 | async-start | bytes 3538944 | tf_op jit(solution)/shard_map/all_gather | solution.py:69
  8.0 211.6 %all-gather.6.cloned.1.call-start = ((), (), s32[]{:S(2)}) async-start(), calls=%async_computation.2 | async-start | bytes 1966080 | tf_op jit(solution)/shard_map/all_gather | solution.py:90
  8.7 242.8 %all-reduce.2.cloned.1.call-start = ((), (), s32[]{:S(2)}) async-start(), calls=%async_computation.5 | async-start | bytes 3145728 | tf_op jit(solution)/shard_map/psum | solution.py:87
  158.8 1.9 copy-start.1
  169.5 1.2 copy-start.2
  190.7 1.9 copy-start.1
  201.4 1.2 copy-start.2
  205.6 1.6 copy-start.4
  205.6 1.8 copy-start.5
  209.8 1.1 copy-start.3
  209.8 205.1 %all-gather.12.cloned.1.call-start = ((), (), s32[]{:S(2)}) async-start(), calls=%async_computation.6 | async-start | bytes 6488064 | tf_op jit(solution)/shard_map/all_gather | solution.py:98
  214.2 208.4 %all-to-all-start = ((bf16[8,1408,256]{1,2,0:T(8,128)(2,1)}), bf16[8,1408,256]{1,2,0:T(8,128)(2,1)}, u32[]{:S(2)}, u32[]{:S(2)}) async-start(bf16[8,1408,256]{1,2,0:T(8,128)(2,1)} %stack.2), calls=%async_computation | async-start | bytes 11534336 | tf_op jit(solution)/shard_map/all_to_all | solution.py:13
  218.9 289.2 %all-gather.14.cloned.1.call-start = ((), (), s32[]{:S(2)}) async-start(), calls=%async_computation.7 | async-start | bytes 6488064 | tf_op jit(solution)/shard_map/all_gather | solution.py:99
  219.5 195.4 %copy-start.6 = (f32[2048]{0:T(1024)S(1)}, f32[2048]{0:T(1024)}, u32[]{:S(2)}) copy-start(f32[2048]{0:T(1024)} %param.20) | copy-start | bytes 24580
  219.5 327.3 %reduce-scatter.2.cloned.1.call-start = ((), (), s32[]{:S(2)}) async-start(), calls=%async_computation.8 | async-start | bytes 1966080 | tf_op jit(solution)/shard_map/reduce_scatter | solution.py:105
Sparse Core Ops, SparseCore 0:
  9.5 62.7 all-gather.7
  74.5 58.6 all-gather.9
  134.7 18.2 all-gather.5
  210.0 41.5 all-reduce.1
  253.6 161.2 all-gather.11
  416.9 91.1 all-gather.13
  520.5 26.2 reduce-scatter.1
